TPU v7x, 32 devices: a whole 2x2x4 slice. The times are simulated.
32 devices in a mesh: dp: 4 (over y, x), kv: 4 (over z), tp: 2 (over core).
Axes of the slice: x: 2, y: 2, z: 4, core: 2. Of those that a mesh axis runs over, the one named last changes fastest.
Arguments:
- pieces: bfloat16 [4096, 8, 2048], P(('kv', 'tp'), 'dp'), parts along dimension 1, may hold values from -6 to 6
- new_tokens: bfloat16 [256, 2048], P(('dp', 'kv', 'tp')), parts along dimension 0, may hold values from -6 to 6
- w_query: bfloat16 [2048, 1024], P(None, 'tp'), may hold values from -0.125 to 0.125
- w_key: bfloat16 [2048, 1024], P(None, 'tp'), may hold values from -0.125 to 0.125
- w_value: bfloat16 [2048, 2048], P(None, 'tp'), may hold values from -0.125 to 0.125
- w_decay: bfloat16 [2048, 1024], P(None, 'tp'), may hold values from -0.125 to 0.125
- decay_bias: float32 [1024], replicated, may hold values from 0 to 9
- norm_gain: float32 [2048], replicated, may hold values from 0.1 to 1.9
- head_gain: float32 [2048], replicated, may hold values from 0.1 to 1.9
- w_out: bfloat16 [2048, 2048], replicated, may hold values from -0.125 to 0.125
- prompt_state: float32 [8, 8, 128, 256], P('dp', 'tp', 'kv'), parts along dimension 0, may hold values from -8 to 8
- decode_state: float32 [256, 8, 128, 256], P(('dp', 'kv'), 'tp'), parts along dimension 0, may hold values from -8 to 8
Outputs:
- mixed_piece: bfloat16 [4096, 8, 2048], P(('kv', 'tp'), 'dp'), parts along dimension 1
- mixed_decode: bfloat16 [256, 2048], P(('dp', 'kv', 'tp')), parts along dimension 0
- prompt_state_out: float32 [8, 8, 128, 256], P('dp', 'tp', 'kv'), parts along dimension 0
- decode_state_out: float32 [256, 8, 128, 256], P(('dp', 'kv'), 'tp'), parts along dimension 0
There are 4 independent parts, one for each index of `dp`. A program takes and returns all parts, laid end to end along the dimension named above; an argument that names none is the same for every part. Nothing has to cross between parts.
All inputs are finite; a program needn't handle non-finite values.
Results may differ from a plain program's by a relative error of at most 0.014.
Values may be sent and summed in bfloat16 or wider, within the bound.
A program may use at most 192 MiB of HBM per device.

v0:
```python
import jax
import jax.numpy as jnp
from jax import lax
from jax.sharding import PartitionSpec as P

DK = 128
DV = 256
BLOCK = 64


highest = lax.Precision.HIGHEST
norm_eps = 0.1
decay_tau = 16.0
part_limit = 16


def entering(value, axis, join, neutral):
    count, mine = (lax.axis_size(axis), lax.axis_index(axis))
    pieces = jax.tree.map(lambda part: lax.all_gather(part, axis), value)
    subtotal = jax.tree.map(
        lambda part, zero: jnp.full_like(part, 0) + jnp.asarray(zero, part.dtype), value, neutral
    )

    def step(position, subtotal):
        longer = join(subtotal, jax.tree.map(lambda part: part[position], pieces))
        return jax.tree.map(lambda new, old: jnp.where(position < mine, new, old), longer, subtotal)

    return lax.fori_loop(0, count - 1, step, subtotal)


def broadcast(block, axis, holder):
    block = jnp.where(lax.axis_index(axis) == holder, block, jnp.zeros_like(block))
    return lax.psum(block, axis)


def rms_rows(row_block, gain):
    wide = row_block.astype(jnp.float32)
    factor = lax.rsqrt(jnp.mean(wide * wide, axis=-1, keepdims=True) + norm_eps)
    return (wide * factor * gain).astype(jnp.bfloat16)


def head_norm(outputs, gain):
    factor = lax.rsqrt(jnp.mean(outputs * outputs, axis=-1, keepdims=True) + norm_eps)
    flat = (outputs * factor).reshape(outputs.shape[:-2] + (-1,))
    return (flat * gain).astype(jnp.bfloat16)


def block_terms(q_blk, k_blk, v_blk, g_blk):
    block_len = q_blk.shape[0]
    part_len = min(part_limit, block_len)
    part_count = block_len // part_len
    within = jnp.cumsum(g_blk, axis=0)
    part_ends = within[part_len - 1 :: part_len]
    anchor = jnp.concatenate([jnp.zeros_like(part_ends[:1]), part_ends[:-1]], axis=0)
    q_wide = q_blk.astype(jnp.float32)
    k_wide = k_blk.astype(jnp.float32)
    q_parts = q_wide.reshape((part_count, part_len) + q_blk.shape[1:])
    w_parts = within.reshape((part_count, part_len) + within.shape[1:])
    near_query = (q_parts * jnp.exp(w_parts - anchor[:, None])).astype(jnp.bfloat16)
    near_key = (k_wide[None] * jnp.exp(anchor[:, None] - within[None])).astype(jnp.bfloat16)
    scores = jnp.einsum(
        "itbhk,isbhk->ibhts", near_query, near_key, preferred_element_type=jnp.float32
    )
    row_pos = jnp.arange(part_count)[:, None] * part_len + jnp.arange(part_len)[None]
    keep = row_pos[:, :, None] >= jnp.arange(block_len)[None, None]
    weights = jnp.where(keep[:, None, None], scores, 0.0).astype(jnp.bfloat16)
    in_block = jnp.einsum("ibhts,sbhv->itbhv", weights, v_blk, preferred_element_type=jnp.float32)
    in_block = in_block.reshape((block_len,) + in_block.shape[2:])
    block_total = within[-1]
    start_query = (q_wide * jnp.exp(within)).astype(jnp.bfloat16)
    end_key = (k_wide * jnp.exp(block_total[None] - within)).astype(jnp.bfloat16)
    added = jnp.einsum("sbhk,sbhv->bhkv", end_key, v_blk, preferred_element_type=jnp.float32)
    return (in_block, start_query, block_total, added)


def block_form(query_all, key_all, value_all, decay_all):
    seq_len, batch_size, head_count, width_k = query_all.shape
    width_v = value_all.shape[-1]
    block_count = seq_len // BLOCK

    def to_blocks(tensor):
        return tensor.reshape((block_count, BLOCK) + tensor.shape[1:])

    def advance(carried, inputs):
        states, offset = carried
        in_block, start_query, block_total, added = block_terms(*inputs)
        new_states = jnp.exp(block_total)[..., None] * states + added
        return ((new_states, offset + block_total), (in_block, start_query, states, offset))

    start_states = jnp.zeros((batch_size, head_count, width_k, width_v), jnp.float32)
    start_log = jnp.zeros((batch_size, head_count, width_k), jnp.float32)
    (local_states, totals), (outputs, start_queries, block_starts, block_offsets) = lax.scan(
        advance,
        (start_states, start_log),
        (to_blocks(query_all), to_blocks(key_all), to_blocks(value_all), to_blocks(decay_all)),
    )
    return (outputs, start_queries, block_starts, block_offsets, local_states, totals)


def single_token(query, key_new, value_new, decay, states):
    query = query.astype(jnp.float32)
    key_new = key_new.astype(jnp.float32)
    value_new = value_new.astype(jnp.float32)
    from_state = jnp.einsum("bhk,bhkv->bhv", query * jnp.exp(decay), states, precision=highest)
    token_score = jnp.sum(query * key_new, axis=-1, keepdims=True)
    outputs = from_state + token_score * value_new
    carried = jnp.exp(decay)[..., None] * states + key_new[..., None] * value_new[..., None, :]
    return (outputs, carried)


def chain(earlier, later):
    return (earlier[0] + later[0], jnp.exp(later[0])[..., None] * earlier[1] + later[1])


def on_device(
    pieces,
    new_tokens,
    w_query,
    w_key,
    w_value,
    w_decay,
    decay_bias,
    norm_gain,
    head_gain,
    w_out,
    prompt_state,
    decode_state,
):
    tp_size = lax.axis_size("tp")
    kv_size = lax.axis_size("kv")
    tp_index = lax.axis_index("tp")
    kv_index = lax.axis_index("kv")
    heads_here = w_query.shape[1] // DK
    bias_here = lax.dynamic_slice_in_dim(decay_bias, tp_index * (heads_here * DK), heads_here * DK)
    gain_here = lax.dynamic_slice_in_dim(head_gain, tp_index * (heads_here * DV), heads_here * DV)
    own_pos, prompt_count, width = pieces.shape
    piece_count = own_pos * prompt_count
    normed_piece = rms_rows(pieces, norm_gain).reshape(piece_count, width)
    normed_dec = rms_rows(new_tokens, norm_gain)
    rows_all = jnp.concatenate([normed_piece, normed_dec], axis=0)
    row_count = rows_all.shape[0]
    row_block = lax.all_gather(rows_all, "tp", axis=0, tiled=True)
    products = jnp.concatenate(
        [
            jnp.dot(row_block, w_query, preferred_element_type=jnp.float32),
            jnp.dot(row_block, w_key, preferred_element_type=jnp.float32),
            jnp.dot(row_block, w_value, preferred_element_type=jnp.float32),
            jnp.dot(row_block, w_decay, preferred_element_type=jnp.float32),
        ],
        axis=-1,
    )
    products = products.reshape(tp_size, row_count, products.shape[-1])
    piece_prod = products[:, :piece_count].reshape(
        tp_size * own_pos, prompt_count, products.shape[-1]
    )
    dec_prod = products[:, piece_count:].reshape(
        tp_size * (row_count - piece_count), products.shape[-1]
    )

    def split_roles(product):
        lead = product.shape[:-1]
        qk_cols = heads_here * DK
        v_cols = heads_here * DV
        queries = (product[..., :qk_cols] * DK ** (-0.5)).astype(jnp.bfloat16)
        keys_new = product[..., qk_cols : 2 * qk_cols].astype(jnp.bfloat16)
        values_new = product[..., 2 * qk_cols : 2 * qk_cols + v_cols].astype(jnp.bfloat16)
        decays = jax.nn.log_sigmoid(product[..., 2 * qk_cols + v_cols :] + bias_here) / decay_tau
        return (
            queries.reshape(lead + (heads_here, DK)),
            keys_new.reshape(lead + (heads_here, DK)),
            values_new.reshape(lead + (heads_here, DV)),
            decays.reshape(lead + (heads_here, DK)),
        )

    query_p, key_p, value_p, decay_p = split_roles(piece_prod)
    in_blocks, start_queries, block_starts, block_offsets, local_states, totals = block_form(
        query_p, key_p, value_p, decay_p
    )
    whole_start = lax.all_gather(
        prompt_state.astype(jnp.bfloat16), "kv", axis=2, tiled=True
    ).astype(prompt_state.dtype)
    prefix_log, prefix_states = entering(
        (totals, local_states), "kv", chain, (jnp.zeros_like(totals), jnp.zeros_like(local_states))
    )
    incoming = jnp.exp(prefix_log)[..., None] * whole_start + prefix_states
    full_starts = block_starts + jnp.exp(block_offsets)[..., None] * incoming[None]
    from_state = jnp.einsum(
        "ntbhk,nbhkv->ntbhv", start_queries.astype(jnp.float32), full_starts, precision=highest
    )
    piece_att = (in_blocks + from_state).reshape((tp_size * own_pos,) + in_blocks.shape[2:])
    rows_k = prompt_state.shape[2]
    final_all = jnp.exp(totals)[..., None] * incoming + local_states
    final_all = broadcast(final_all.astype(jnp.bfloat16), "kv", kv_size - 1).astype(final_all.dtype)
    prompt_out = lax.dynamic_slice_in_dim(final_all, kv_index * rows_k, rows_k, 2)
    query_d, key_d, value_d, decay_d = split_roles(dec_prod)
    decode_att, decode_out = single_token(query_d, key_d, value_d, decay_d, decode_state)
    piece_normed = head_norm(piece_att, gain_here)
    dec_normed = head_norm(decode_att, gain_here)
    send_rows = jnp.concatenate(
        [
            piece_normed.reshape(tp_size, piece_count, piece_normed.shape[-1]),
            dec_normed.reshape(tp_size, dec_normed.shape[0] // tp_size, dec_normed.shape[-1]),
        ],
        axis=1,
    )
    mixed = jnp.dot(
        lax.all_to_all(send_rows, "tp", split_axis=0, concat_axis=2, tiled=True),
        w_out,
        preferred_element_type=jnp.float32,
    ).astype(jnp.bfloat16)
    mixed_piece = mixed[0, :piece_count].reshape(own_pos, prompt_count, mixed.shape[-1])
    mixed_decode = mixed[0, piece_count:]
    return (mixed_piece, mixed_decode, prompt_out, decode_out)


def solution(mesh):
    return jax.shard_map(
        on_device,
        mesh=mesh,
        in_specs=(
            P(("kv", "tp"), "dp", None),
            P(("dp", "kv", "tp"), None),
            P(None, "tp"),
            P(None, "tp"),
            P(None, "tp"),
            P(None, "tp"),
            P(),
            P(),
            P(),
            P(),
            P("dp", "tp", "kv", None),
            P(("dp", "kv"), "tp", None, None),
        ),
        out_specs=(
            P(("kv", "tp"), "dp", None),
            P(("dp", "kv", "tp"), None),
            P("dp", "tp", "kv", None),
            P(("dp", "kv"), "tp", None, None),
        ),
        check_vma=False,
    )
```

profile of v0, /device:TPU:0, one launch (start us, length us, event | category | flops | bytes accessed | tf_op | source)
XLA Modules:
  0.0 593.3 jit_solution(7355027402544248402)
XLA Ops:
  8.3 6.6 %fusion.32 = f32[512,2]{1,0:T(8,128)S(1)} fusion(bf16[512,2,2048]{2,1,0:T(2,128)(2,1)} %param.16), kind=kLoop, calls=%fused_computation.52 | loop fusion | flops 6290432 | bytes 4198400 | tf_op jit(solution)/shard_map/reduce_sum | solution.py:38
  15.0 8.7 %fusion.34 = bf16[512,2,2048]{2,1,0:T(2,128)(2,1)} fusion(bf16[512,2,2048]{2,1,0:T(2,128)(2,1)} %param.16, f32[2048]{0:T(1024)S(1)} %copy-done.10, f32[512,2]{1,0:T(8,128)S(1)} %add_rsqrt_fusion), kind=kLoop, calls=%fused_computation.54 | loop fusion | flops 8388608 | bytes 8400896 | tf_op jit(solution)/shard_map/convert_element_type | solution.py:39
  23.8 7.2 %reshape.184 = bf16[1024,2048]{1,0:T(8,128)(2,1)} reshape(bf16[512,2,2048]{2,1,0:T(2,128)(2,1)} %fusion.34) | data formatting | bytes 8388608 | tf_op jit(solution)/shard_map/reshape | solution.py:138
  31.0 4.8 pad_maximum_fusion.1
  36.5 22.8 %all-gather.5.cloned.1.call-done = bf16[2064,2048]{1,0:T(8,128)(2,1)} async-done(((bf16[1032,2048]{1,0:T(8,128)(2,1)}), bf16[2064,2048]{1,0:T(8,128)(2,1)}) %all-gather.5.cloned.1.call-update) | async-done | bytes 8454160 | tf_op jit(solution)/shard_map/all_gather | solution.py:142
  59.4 9.6 %fusion.61 = f32[2064,512]{1,0:T(8,128)} fusion(bf16[2064,2048]{1,0:T(8,128)(2,1)} %all-gather.5.cloned.1.call-done, bf16[2048,512]{1,0:T(8,128)(2,1)S(1)} %copy-done), kind=kOutput, calls=%fused_computation.109 | convolution fusion | flops 4328521728 | bytes 14778368 | tf_op jit(solution)/shard_map/dot_general | solution.py:148
  69.0 11.2 %fusion.60 = f32[2064,1024]{1,0:T(8,128)} fusion(bf16[2064,2048]{1,0:T(8,128)(2,1)S(1)} %copy-done.13, bf16[2048,1024]{1,0:T(8,128)(2,1)S(1)} %copy-done.14), kind=kOutput, calls=%fused_computation.108 | convolution fusion | flops 8657043456 | bytes 21102592 | tf_op jit(solution)/shard_map/dot_general | solution.py:147
  80.2 6.1 %fusion.59 = f32[2064,512]{1,0:T(8,128)} fusion(bf16[2064,2048]{1,0:T(8,128)(2,1)S(1)} %copy-done.13, bf16[2048,512]{1,0:T(8,128)(2,1)S(1)} %copy-done.15), kind=kOutput, calls=%fused_computation.107 | convolution fusion | flops 4328521728 | bytes 14778368 | tf_op jit(solution)/shard_map/dot_general | solution.py:146
  86.3 6.1 %fusion.58 = f32[2064,512]{1,0:T(8,128)} fusion(bf16[2064,2048]{1,0:T(8,128)(2,1)S(1)} %copy-done.13, bf16[2048,512]{1,0:T(8,128)(2,1)S(1)} %copy-done.16), kind=kOutput, calls=%fused_computation.106 | convolution fusion | flops 4328521728 | bytes 14778368 | tf_op jit(solution)/shard_map/dot_general | solution.py:145
  92.4 8.1 %pad_maximum_fusion = f32[2064,2560]{1,0:T(8,128)S(1)} fusion(f32[2064,512]{1,0:T(8,128)} %fusion.61, f32[2064,1024]{1,0:T(8,128)} %fusion.60, f32[2064,512]{1,0:T(8,128)} %fusion.59, f32[2064,512]{1,0:T(8,128)} %fusion.58), kind=kLoop, calls=%fused_computation.45 | loop fusion | flops 15851520 | bytes 42270720 | tf_op jit(solution)/shard_map/concatenate | solution.py:143
  100.5 7.0 %copy-done.4 = f32[2064,2560]{1,0:T(8,128)} copy-done((f32[2064,2560]{1,0:T(8,128)}, f32[2064,2560]{1,0:T(8,128)S(1)}, u32[]{:S(2)}) %copy-start.4) | copy-done | bytes 21135384
  107.5 7.8 %slice.66 = f32[2,1024,2560]{2,1,0:T(8,128)} slice(f32[2,1032,2560]{2,1,0:T(8,128)S(1)} %bitcast.117), slice={[0:2], [0:1024], [0:2560]} | slice | bytes 41943040 | tf_op jit(solution)/shard_map/slice | solution.py:153
  115.3 24.3 %reshape.186 = f32[1024,2,2560]{2,1,0:T(2,128)} reshape(f32[2,1024,2560]{2,1,0:T(8,128)} %slice.66) | data formatting | bytes 41943040 | tf_op jit(solution)/shard_map/reshape | solution.py:153
  139.7 9.1 %convert.14 = bf16[1024,2,2560]{2,1,0:T(2,128)(2,1)S(1)} convert(f32[1024,2,2560]{2,1,0:T(2,128)} %reshape.186) | non-fusion elementwise | flops 5242880 | bytes 31457280 | tf_op jit(solution)/shard_map/convert.9
  148.8 3.9 copy-done.5
  152.7 7.0 %slice.69 = bf16[1024,2,1024]{2,1,0:T(2,128)(2,1)} slice(bf16[1024,2,2560]{2,1,0:T(2,128)(2,1)} %copy-done.5), slice={[0:1024], [0:2], [1024:2048]} | slice | bytes 8388608 | tf_op jit(solution)/shard_map/slice | solution.py:166
  159.8 14.1 %fusion.40 = (bf16[1024,2,512]{2,1,0:T(2,128)(2,1)}, f32[1024,2,512]{2,1,0:T(2,128)}) fusion(f32[1024,2,2560]{2,1,0:T(2,128)} %reshape.186, f32[512]{0:T(512)S(1)} %dynamic_slice.38), kind=kLoop, calls=%fused_computation.68 | loop fusion | flops 12582912 | bytes 14682112 | tf_op jit(solution)/shard_map/convert_element_type | solution.py:164
  173.9 7.1 %reshape_reshape.12 = f32[16,64,2,4,128]{4,3,2,1,0:T(4,128)} reshape(f32[1024,2,512]{2,1,0:T(2,128)} %get-tuple-element.350) | data formatting | bytes 8388608 | tf_op jit(solution)/shard_map/reshape;reshape | solution.py:82
  181.0 2.6 reshape_reshape.13
  183.6 7.7 %reshape.204 = bf16[16,64,2,4,256]{4,3,2,1,0:T(4,128)(2,1)} reshape(bf16[1024,2,1024]{2,1,0:T(2,128)(2,1)} %slice.69) | data formatting | bytes 8388608 | tf_op jit(solution)/shard_map/reshape;reshape | solution.py:82
  191.3 2.6 reshape_reshape.15
  194.0 145.8 %while.37 = (s32[]{:T(128)}, f32[2,4,128,256]{3,2,1,0:T(8,128)S(1)}, f32[2,4,128]{2,1,0:T(4,128)S(1)}, f32[16,64,2,4,256]{4,1,3,2,0:T(8,128)}, bf16[16,64,2,4,12...) while((s32[]{:T(128)}, ...), condition=%wide.region_4.5_spmd.clone, body=%wide.region_2.4_spmd.clone.sunk | while | flops 65543236 | bytes 11581150 | solution.py:92
  194.0 1.1 bitcast_dynamic-update-slice_fusion.4
  195.1 1.1 fusion.87
  204.2 1.1 fusion.87
  213.3 1.1 fusion.87
  222.4 1.1 fusion.87
  230.4 1.1 bitcast_dynamic-update-slice_fusion.4
  231.5 1.1 fusion.87
  240.6 1.1 fusion.87
  249.7 1.1 fusion.87
  258.8 1.1 fusion.87
  266.8 1.1 bitcast_dynamic-update-slice_fusion.4
  285.0 1.1 bitcast_dynamic-update-slice_fusion.4
  294.1 1.2 bitcast_dynamic-update-slice_fusion.4
  303.3 1.1 bitcast_dynamic-update-slice_fusion.4
  321.5 1.1 bitcast_dynamic-update-slice_fusion.4
  330.6 1.1 bitcast_dynamic-update-slice_fusion.4
  340.9 19.8 %all_gather.23 = bf16[2,4,128,256]{3,2,1,0:T(8,128)(2,1)} all-gather(bf16[2,4,32,256]{3,2,1,0:T(8,128)(2,1)S(1)} %convert_element_type.113), channel_id=1, replica_groups=mesh['dp'=4,'kv'=4,'tp'=2] {'kv'}, dimensions={2}, use_global_device_ids=true | all-gather | bytes 655360 | tf_op jit(solution)/shard_map/all_gather | solution.py:179
  362.8 6.4 %fusion.62 = f32[16,4,1,256]{3,2,1,0:T(1,128)S(1)} fusion(f32[16,4,128,1]{2,3,1,0:T(1,128)S(1)} %bitcast.127, f32[16,4,128,256]{3,2,1,0:T(8,128)} %param.27), kind=kOutput, calls=%fused_computation.110 | convolution fusion | flops 25165824 | bytes 8486912 | tf_op jit(solution)/shard_map/bhk,bhkv->bhv/dot_general | solution.py:104
  369.6 13.8 %all-gather = f32[8,4,128]{2,1,0:T(4,128)S(1)} all-gather(f32[2,4,128]{2,1,0:T(4,128)S(1)} %get-tuple-element.179), channel_id=2, replica_groups=mesh['dp'=4,'kv'=4,'tp'=2] {'kv'}, dimensions={0}, use_global_device_ids=true | all-gather | bytes 20480 | tf_op jit(solution)/shard_map/all_gather | solution.py:19
  383.4 8.4 %multiply_add_fusion = f32[16,4,128,256]{3,2,1,0:T(8,128)} fusion(f32[16,4,128,256]{3,2,1,0:T(8,128)} %param.27, f32[16,4,256]{2,1,0:T(4,128)S(1)} %reshape.195, f32[16,4,128]{2,1,0:T(4,128)S(1)} %reshape.194, f32[16,4,128]{2,1,0:T(4,128)S(1)} %exp.75), kind=kLoop, calls=%fused_computation.56 | loop fusion | flops 6291456 | bytes 16908288 | tf_op jit(solution)/shard_map/add | solution.py:107
  391.7 33.7 %all-gather.7.cloned.1.call-done = f32[8,4,128,256]{3,2,1,0:T(8,128)} async-done(((f32[2,4,128,256]{3,2,1,0:T(8,128)}), f32[8,4,128,256]{3,2,1,0:T(8,128)}) %all-gather.7.cloned.1.call-update) | async-done | bytes 4194320 | tf_op jit(solution)/shard_map/all_gather | solution.py:19
  425.5 5.1 while.38
  425.5 1.7 fusion.89
  427.2 1.6 fusion.89
  428.9 1.6 fusion.89
  430.6 2.3 fusion.44
  432.8 15.8 %multiply_reduce_fusion = (f32[16,64,2,4]{1,3,2,0:T(4,128)S(1)}, f32[16,64,2,4,256]{4,1,3,2,0:T(8,128)}) fusion(f32[16,64,2,4,256]{4,1,3,2,0:T(8,128)} %get-tuple-element.176, bf16[16,64,2,4,128]{4,1,3,2,0:T(8,128)(2,1)} %get-tuple-element.183, f32[16,2,4,128,256]{4,3,2,1,0:T(8,128)} %get-tuple-element.177, f32[2,4,128,256]{3,2,1,0:T(8,128)S(1)} %get-tuple-element.342, ...), kind=kOutput, calls=%fused_computation.58 | convolution fusion | flops 3235897344 | bytes 36798464 | tf_op jit(solution)/shard_map/ntbhk,nbhkv->ntbhv/dot_general | solution.py:187
  448.7 12.2 %copy.91 = f32[16,64,2,4,256]{4,3,2,1,0:T(4,128)} copy(f32[16,64,2,4,256]{4,1,3,2,0:T(8,128)} %get-tuple-element.356) | data formatting | bytes 16777216 | tf_op jit(solution)/shard_map/add | solution.py:190
  460.9 10.9 %reshape.187 = f32[2,1024,1024]{2,1,0:T(8,128)} reshape(f32[16,64,2,4,256]{4,3,2,1,0:T(4,128)} %copy.91) | data formatting | bytes 16777216 | tf_op jit(solution)/shard_map/reshape | solution.py:190
  472.5 4.5 mul.244
  477.0 10.7 %mul.245 = f32[2,1024,1024]{2,1,0:T(8,128)} reshape(f32[1024,2,4,256]{3,2,1,0:T(4,128)} %mul.244) | data formatting | bytes 16777216 | tf_op jit(solution)/shard_map/mul | solution.py:44
  487.8 8.1 %multiply_convert_fusion.4 = bf16[2,1024,1024]{2,1,0:T(8,128)(2,1)S(1)} fusion(f32[2,1024,1024]{2,1,0:T(8,128)} %reshape.187, f32[2,1024,1024]{2,1,0:T(8,128)} %mul.245, f32[1024]{0:T(1024)S(1)} %dynamic_slice.39), kind=kLoop, calls=%fused_computation.57 | loop fusion | flops 6291456 | bytes 20975616 | tf_op jit(solution)/shard_map/convert_element_type | solution.py:45
  496.3 7.1 %all_to_all.15 = bf16[2,1032,1024]{2,1,0:T(8,128)(2,1)S(1)} all-to-all(bf16[2,1032,1024]{2,1,0:T(8,128)(2,1)S(1)} %pad_maximum_fusion.2), channel_id=1, replica_groups=mesh['dp'=4,'kv'=4,'tp'=2] {'tp'}, dimensions={0} | all-to-all | bytes 8454144 | tf_op jit(solution)/shard_map/all_to_all | solution.py:207
  503.4 40.2 %copy.94 = bf16[1,1032,2,1024]{3,2,1,0:T(2,128)(2,1)S(1)} copy(bf16[1,1032,2,1024]{3,1,2,0:T(8,128)(2,1)S(1)} %bitcast.122) | data formatting | bytes 8454144 | tf_op jit(solution)/shard_map/all_to_all | solution.py:207
  543.6 3.7 copy.105
  547.3 12.7 %fusion.37 = bf16[1,1032,2048]{2,1,0:T(8,128)(2,1)S(1)} fusion(bf16[1032,2048]{1,0:T(8,128)(2,1)} %bitcast.125, bf16[2048,2048]{1,0:T(8,128)(2,1)} %param.25), kind=kOutput, calls=%fused_computation.62 | convolution fusion | flops 8659156992 | bytes 16842752 | tf_op jit(solution)/shard_map/dot_general | solution.py:206
  560.0 2.0 copy-done.7
  562.0 2.3 slice.76
  564.3 7.6 %reshape_squeeze.3 = bf16[512,2,2048]{2,1,0:T(2,128)(2,1)} reshape(bf16[1,1024,2048]{2,1,0:T(8,128)(2,1)} %slice.76) | data formatting | bytes 8388608 | tf_op jit(solution)/shard_map/reshape;squeeze | solution.py:211
  571.9 1.4 slice_bitcast_fusion.2
  573.3 11.6 %all-reduce.3.cloned.1.call-done = bf16[2,4,128,256]{3,2,1,0:T(8,128)(2,1)} async-done(((bf16[2,4,128,256]{3,2,1,0:T(8,128)(2,1)}), bf16[2,4,128,256]{3,2,1,0:T(8,128)(2,1)}) %all-reduce.3.cloned.1.call-update) | async-done | bytes 524304 | tf_op jit(solution)/shard_map/psum | solution.py:33
  584.9 1.6 dynamic-slice_convert_fusion.1
  (414 shorter events, 133.1 us)
Async XLA Ops:
  7.2 52.2 %copy-start = (bf16[2048,512]{1,0:T(8,128)(2,1)S(1)}, bf16[2048,512]{1,0:T(8,128)(2,1)}, u32[]{:S(2)}) copy-start(bf16[2048,512]{1,0:T(8,128)(2,1)} %param.21) | copy-start | bytes 6291460
  7.2 7.7 %copy-start.9 = (bf16[8,2048]{1,0:T(8,128)(2,1)S(1)}, bf16[8,2048]{1,0:T(8,128)(2,1)}, u32[]{:S(2)}) copy-start(bf16[8,2048]{1,0:T(8,128)(2,1)} %param.17) | copy-start | bytes 98308
  7.2 7.7 %copy-start.10 = (f32[2048]{0:T(1024)S(1)}, f32[2048]{0:T(1024)}, u32[]{:S(2)}) copy-start(f32[2048]{0:T(1024)} %param.23) | copy-start | bytes 24580
  7.2 52.1 %all-gather.5.cloned.1.call-start = ((), (), s32[]{:S(2)}) async-start(), calls=%async_computation.1 | async-start | bytes 12681216 | tf_op jit(solution)/shard_map/all_gather | solution.py:142
  35.8 0.7 copy-start.12
  35.8 389.7 %all-gather.7.cloned.1.call-start = ((), (), s32[]{:S(2)}) async-start(), calls=%async_computation.3 | async-start | bytes 5242880 | tf_op jit(solution)/shard_map/all_gather | solution.py:19
  59.4 9.7 %copy-start.13 = (bf16[2064,2048]{1,0:T(8,128)(2,1)S(1)}, bf16[2064,2048]{1,0:T(8,128)(2,1)}, u32[]{:S(2)}) copy-start(bf16[2064,2048]{1,0:T(8,128)(2,1)} %all-gather.5.cloned.1.call-done) | copy-start | bytes 25362436
  59.4 9.7 %copy-start.14 = (bf16[2048,1024]{1,0:T(8,128)(2,1)S(1)}, bf16[2048,1024]{1,0:T(8,128)(2,1)}, u32[]{:S(2)}) copy-start(bf16[2048,1024]{1,0:T(8,128)(2,1)} %param.20) | copy-start | bytes 12582916
  69.0 11.2 %copy-start.15 = (bf16[2048,512]{1,0:T(8,128)(2,1)S(1)}, bf16[2048,512]{1,0:T(8,128)(2,1)}, u32[]{:S(2)}) copy-start(bf16[2048,512]{1,0:T(8,128)(2,1)} %param.19) | copy-start | bytes 6291460
  80.2 6.1 %copy-start.16 = (bf16[2048,512]{1,0:T(8,128)(2,1)S(1)}, bf16[2048,512]{1,0:T(8,128)(2,1)}, u32[]{:S(2)}) copy-start(bf16[2048,512]{1,0:T(8,128)(2,1)} %param.18) | copy-start | bytes 6291460
  100.5 7.1 %copy-start.4 = (f32[2064,2560]{1,0:T(8,128)}, f32[2064,2560]{1,0:T(8,128)S(1)}, u32[]{:S(2)}) copy-start(f32[2064,2560]{1,0:T(8,128)S(1)} %pad_maximum_fusion) | copy-start | bytes 63406084
  148.8 4.0 copy-start.5
  173.9 7.1 %slice-start = ((bf16[1024,2,2560]{2,1,0:T(2,128)(2,1)}), bf16[1024,2,512]{2,1,0:T(2,128)(2,1)S(1)}, s32[]{:S(2)}) async-start(bf16[1024,2,2560]{2,1,0:T(2,128)(2,1)} %copy-done.5), calls=%async_computation.4 | async-start | bytes 4194304 | tf_op jit(solution)/shard_map/slice | solution.py:165
  183.6 7.7 %copy-start.6 = (bf16[1024,2,512]{2,1,0:T(2,128)(2,1)S(1)}, bf16[1024,2,512]{2,1,0:T(2,128)(2,1)}, u32[]{:S(2)}) copy-start(bf16[1024,2,512]{2,1,0:T(2,128)(2,1)} %get-tuple-element.349) | copy-start | bytes 6291460
  193.9 146.9 %copy-start.8 = (f32[2,4,32,256]{3,2,1,0:T(8,128)S(1)}, f32[2,4,32,256]{3,2,1,0:T(8,128)}, u32[]{:S(2)}) copy-start(f32[2,4,32,256]{3,2,1,0:T(8,128)} %param.26) | copy-start | bytes 786436
  193.9 146.9 %copy-start.11 = (f32[2048]{0:T(1024)S(1)}, f32[2048]{0:T(1024)}, u32[]{:S(2)}) copy-start(f32[2048]{0:T(1024)} %param.24) | copy-start | bytes 24580
  339.7 1.0 copy-start.2
  340.7 244.2 %all-reduce.3.cloned.1.call-start = ((), (), s32[]{:S(2)}) async-start(), calls=%async_computation.2 | async-start | bytes 1048576 | tf_op jit(solution)/shard_map/psum | solution.py:33
  425.5 5.1 copy-start.3
  560.0 2.0 copy-start.7
  562.0 24.6 %copy-start.1 = (bf16[2048,512]{1,0:T(8,128)(2,1)S(1)}, bf16[2048,512]{1,0:T(8,128)(2,1)}, u32[]{:S(2)}) copy-start(bf16[2048,512]{1,0:T(8,128)(2,1)} %param.21) | copy-start | bytes 6291460
Sparse Core Ops, SparseCore 0:
  35.9 23.3 all-gather.4
  340.8 84.5 all-gather.6
  547.5 37.4 all-reduce.2
where the time goes:
time: 604 us; the launch traced here: 593 us
  local copies, waits for them, and re-layouts  220 us (36%)
  other arithmetic  163 us (27%)
  matrix products  85 us (14%)
  waiting for transfers between devices  68.3 us (11%)
  blocking collectives  40.7 us (7%)
  between operations  14.3 us (2%)
    all_to_all x1, local copies, waits for them, and re-layouts, on_device(): lax.all_to_all(send_rows, 'tp', split_axis=0, concat_axis=2, tiled=True)  40.2 us
    all_gather x1, waiting for transfers between devices, entering(): pieces = jax.tree.map(lambda part: lax.all_gather(part, axis), value)  33.7 us
    reshape x1, local copies, waits for them, and re-layouts, on_device(): products[:, :piece_count]  24.3 us
    dynamic_update_slice x32, local copies, waits for them, and re-layouts, block_form(): lax.scan(advance, (start_states, start_log), (to_blocks(query_all), to_bl...  24.2 us
    all_gather x1, waiting for transfers between devices, on_device(): row_block = lax.all_gather(rows_all, 'tp', axis=0, tiled=True)  22.8 us
    another operation x4, local copies, waits for them, and re-layouts, to_blocks(): return tensor.reshape((block_count, BLOCK) + tensor.shape[1:])  20.1 us
    all_gather x1, blocking collectives, on_device(): lax.all_gather(prompt_state.astype(jnp.bfloat16), 'kv', axis=2, tiled=True)  19.8 us
    dynamic_update_slice x32, other arithmetic, block_form(): lax.scan(advance, (start_states, start_log), (to_blocks(query_all), to_bl...  17.8 us
  transfers between devices with their start and end apart: 3, of which 3 were waited for; matrix products, arithmetic and copies ran while one was open for 7% of the time, Pallas kernels for 0%

commit v1 on v0

v1 whole, which is shorter than its diff:
```python
import functools

import jax
import jax.numpy as jnp
import numpy as np
from jax import lax
from jax.experimental import pallas as pl
from jax.experimental.pallas import tpu as pltpu
from jax.sharding import PartitionSpec as P

DK = 128
DV = 256
STEP = 64
PART = 16

norm_eps = 0.1
decay_tau = 16.0
f32, bf16 = jnp.float32, jnp.bfloat16
MESH = pl.DeviceIdType.MESH
PAD = 16


def dot(a, b):
    return jnp.dot(a, b, preferred_element_type=f32)


def dot_nt(a, b):
    return lax.dot_general(a, b, (((1,), (1,)), ((), ())), preferred_element_type=f32)


def dot_tn(a, b):
    return lax.dot_general(a, b, (((0,), (0,)), ((), ())), preferred_element_type=f32)


def sum_matrices(prompts):
    n = STEP * prompts
    r, c = np.arange(n)[:, None], np.arange(n)[None]
    same = (r % prompts) == (c % prompts)

    def from_anchor(edge):
        return (same & (c >= edge) & (c <= r)) * 1.0 - (same & (c < edge) & (c > r)) * 1.0

    b = (same & (c <= r)) * 1.0
    rest = (same & (c > r)) * 1.0
    d0 = from_anchor(PART * prompts)[: n // 2]
    d1 = from_anchor(3 * PART * prompts)
    one = np.concatenate([b, rest, d0, d1], axis=0)
    return np.concatenate([one, one, one], axis=1)


def meet_partner(other):
    barrier = pltpu.get_barrier_semaphore()
    pl.semaphore_signal(barrier, inc=1, device_id={"tp": other}, device_id_type=MESH)
    pl.semaphore_wait(barrier, 1)


def front_kernel(
    own, chunk, prompts, heads,
    x_hbm, dec_ref, wq_hbm, wk_hbm, wv_hbm, wd_hbm, bias_ref, gain_ref, mats_ref,
    out_ref, qt_ref, st_ref, tot_ref, dp_ref,
    xb, nb, nd, wq, wk, wv, wd, qs, ks, vs, gs,
    x_sem, w_sem, send_sem, recv_sem, dsend, drecv,
):
    me = lax.axis_index("tp")
    other = 1 - me
    count = own // chunk
    for j in range(count):
        pltpu.make_async_copy(x_hbm.at[pl.ds(j * chunk, chunk)], xb.at[pl.ds(j * chunk, chunk)], x_sem.at[j]).start()
    loads = [
        pltpu.make_async_copy(src, dst, w_sem.at[i])
        for i, (src, dst) in enumerate(((wq_hbm, wq), (wk_hbm, wk), (wv_hbm, wv), (wd_hbm, wd)))
    ]
    for load in loads:
        load.start()
    meet_partner(other)

    def normed(rows):
        wide = rows.astype(f32)
        factor = lax.rsqrt(jnp.mean(wide * wide, axis=-1, keepdims=True) + norm_eps)
        return (wide * factor * gain_ref[...]).astype(bf16)

    def piece_copy(j):
        rows = pl.ds(pl.multiple_of(me * own + j * chunk, chunk), chunk)
        return pltpu.make_async_remote_copy(
            src_ref=nb.at[rows], dst_ref=nb.at[rows], send_sem=send_sem.at[j], recv_sem=recv_sem.at[j],
            device_id={"tp": other}, device_id_type=MESH,
        )

    mine = pl.ds(pl.multiple_of(me * PAD, PAD), PAD)
    nd[mine, :] = normed(dec_ref[...])
    dec_copy = pltpu.make_async_remote_copy(
        src_ref=nd.at[mine], dst_ref=nd.at[mine], send_sem=dsend, recv_sem=drecv,
        device_id={"tp": other}, device_id_type=MESH,
    )
    small = min(64, chunk)
    for j in range(count):
        pltpu.make_async_copy(x_hbm.at[pl.ds(j * chunk, chunk)], xb.at[pl.ds(j * chunk, chunk)], x_sem.at[j]).wait()

        @pl.loop(0, chunk // small)
        def _(s):
            at = j * chunk + s * small
            nb[pl.ds(pl.multiple_of(me * own + at, small), small), :] = normed(xb[pl.ds(pl.multiple_of(at, small), small), :])

        if j == 0:
            dec_copy.start()
        else:
            piece_copy(j - 1).start()
    piece_copy(count - 1).start()
    for load in loads:
        load.wait()

    def decay_of(product):
        t = product + bias_ref[...]
        return (jnp.minimum(t, 0.0) - jnp.log1p(jnp.exp(-jnp.abs(t)))) * (1.0 / decay_tau)

    def project(at):
        rows = pl.ds(pl.multiple_of(at, chunk), chunk)
        block = nb[rows, :]
        qs[rows, :] = (dot(block, wq[...]) * DK ** (-0.5)).astype(bf16)
        ks[rows, :] = dot(block, wk[...]).astype(bf16)
        half = wv.shape[1] // 2
        vs[rows, :half] = dot(block, wv[:, :half]).astype(bf16)
        vs[rows, half:] = dot(block, wv[:, half:]).astype(bf16)
        gs[rows, :] = decay_of(dot(block, wd[...]))

    @pl.loop(0, count)
    def _(j):
        project(me * own + j * chunk)

    @pl.loop(0, count)
    def _(j):
        rows = pl.ds(pl.multiple_of(other * own + j * chunk, chunk), chunk)
        pltpu.make_async_remote_copy(
            src_ref=nb.at[rows], dst_ref=nb.at[rows], send_sem=send_sem.at[j], recv_sem=recv_sem.at[j],
            device_id={"tp": other}, device_id_type=MESH,
        ).wait_recv()
        project(other * own + j * chunk)

    for j in range(count):
        piece_copy(j).wait_send()
    dec_copy.wait()
    dec_rows = nd[...]
    qk = wq.shape[1]
    dp_ref[:, :qk] = (dot(dec_rows, wq[...]) * DK ** (-0.5)).astype(bf16).astype(f32)
    dp_ref[:, qk : 2 * qk] = dot(dec_rows, wk[...]).astype(bf16).astype(f32)
    dp_ref[:, 2 * qk : 3 * qk] = decay_of(dot(dec_rows, wd[...]))
    dp_ref[:, 3 * qk :] = dot(dec_rows, wv[...]).astype(bf16).astype(f32)

    n = STEP * prompts
    half = n // 2
    st_ref[...] = jnp.zeros_like(st_ref)
    tot_ref[...] = jnp.zeros_like(tot_ref)

    @pl.loop(0, 2 * own // n)
    def _(i):
        rows = pl.ds(pl.multiple_of(i * n, n), n)
        g = gs[rows, :]
        hi = g.astype(bf16)
        left = g - hi.astype(f32)
        mid = left.astype(bf16)
        low = (left - mid.astype(f32)).astype(bf16)
        sums = dot(mats_ref[...], jnp.concatenate([hi, mid, low], axis=0))
        b, rest = sums[:n], sums[n : 2 * n]
        d0, d1 = sums[2 * n : 2 * n + half], sums[2 * n + half :]
        q = qs[rows, :].astype(f32)
        k = ks[rows, :].astype(f32)
        row_prompt = lax.broadcasted_iota(jnp.int32, (n, 1), 0) % prompts
        offset = tot_ref[0:1, :]
        for p in range(1, prompts):
            offset = jnp.where(row_prompt == p, tot_ref[p : p + 1, :], offset)
        qt_ref[rows, :] = (q * jnp.exp(b + offset)).astype(bf16)
        start_query = (q * jnp.exp(b)).astype(bf16)
        end_key = (k * jnp.exp(rest)).astype(bf16)
        near_q0 = (q[:half] * jnp.exp(d0)).astype(bf16)
        near_k0 = (k[:half] * jnp.exp(-d0)).astype(bf16)
        near_q1 = (q[half:] * jnp.exp(d1[half:])).astype(bf16)
        near_k1 = (k * jnp.exp(-d1)).astype(bf16)
        block_total = b[n - prompts :]
        decay = jnp.exp(block_total)
        tot_ref[:prompts, :] = tot_ref[:prompts, :] + block_total
        r_at = lax.broadcasted_iota(jnp.int32, (n, n), 0)
        c_at = lax.broadcasted_iota(jnp.int32, (n, n), 1)
        keep = (c_at <= r_at) & (r_at % prompts == c_at % prompts)
        for h in range(heads):
            kc = slice(h * DK, (h + 1) * DK)
            v = vs[rows, h * DV : (h + 1) * DV]
            w0 = jnp.where(keep[:half, :half], dot_nt(near_q0[:, kc], near_k0[:, kc]), 0.0).astype(bf16)
            w1 = jnp.where(keep[half:], dot_nt(near_q1[:, kc], near_k1[:, kc]), 0.0).astype(bf16)
            inner = jnp.concatenate([dot(w0, v[:half]), dot(w1, v)], axis=0)
            state = st_ref[h]
            from_all = dot_nt(start_query[:, kc], state.astype(bf16))
            from_state = from_all[:, :DV]
            for p in range(1, prompts):
                from_state = jnp.where(row_prompt == p, from_all[:, p * DV : (p + 1) * DV], from_state)
            out_ref[rows, h * DV : (h + 1) * DV] = (inner + from_state).astype(bf16)
            zero = jnp.zeros_like(v)
            v_each = jnp.concatenate([jnp.where(row_prompt == p, v, zero) for p in range(prompts)], axis=1)
            added = dot_tn(v_each, end_key[:, kc])
            for p in range(prompts):
                at = slice(p * DV, (p + 1) * DV)
                st_ref[h, at, :] = state[at] * decay[p : p + 1, kc] + added[at]


def back_kernel(
    own, chunk, prompts, heads,
    out_ref, qt_ref, in_ref, gain_ref, dec_ref, w_hbm,
    y_ref, yd_ref,
    w, nl, nr, dl, dr,
    w_sem, send_sem, recv_sem, dsend, drecv,
):
    me = lax.axis_index("tp")
    other = 1 - me
    count = own // chunk
    load = pltpu.make_async_copy(w_hbm, w, w_sem)
    load.start()
    meet_partner(other)

    def head_norm(part, h):
        factor = lax.rsqrt(jnp.mean(part * part, axis=-1, keepdims=True) + norm_eps)
        return (part * factor * gain_ref[:, h * DV : (h + 1) * DV]).astype(bf16)

    def finish(at):
        rows = pl.ds(pl.multiple_of(at, chunk), chunk)
        row_prompt = lax.broadcasted_iota(jnp.int32, (chunk, 1), 0) % prompts
        for h in range(heads):
            cols = slice(h * DV, (h + 1) * DV)
            from_all = dot_nt(qt_ref[rows, h * DK : (h + 1) * DK], in_ref[h])
            from_state = from_all[:, :DV]
            for p in range(1, prompts):
                from_state = jnp.where(row_prompt == p, from_all[:, p * DV : (p + 1) * DV], from_state)
            nl[rows, cols] = head_norm(out_ref[rows, cols].astype(f32) + from_state, h)

    def copy(j):
        src = pl.ds(pl.multiple_of(other * own + j * chunk, chunk), chunk)
        return pltpu.make_async_remote_copy(
            src_ref=nl.at[src], dst_ref=nr.at[pl.ds(j * chunk, chunk)], send_sem=send_sem.at[j], recv_sem=recv_sem.at[j],
            device_id={"tp": other}, device_id_type=MESH,
        )

    for h in range(heads):
        cols = slice(h * DV, (h + 1) * DV)
        dl[:, cols] = head_norm(dec_ref[:, cols], h)
    dec_copy = pltpu.make_async_remote_copy(
        src_ref=dl.at[pl.ds(pl.multiple_of(other * PAD, PAD), PAD)], dst_ref=dr, send_sem=dsend, recv_sem=drecv,
        device_id={"tp": other}, device_id_type=MESH,
    )
    for j in range(count):
        finish(other * own + j * chunk)
        if j == 0:
            dec_copy.start()
        else:
            copy(j - 1).start()
    finish(me * own)
    copy(count - 1).start()

    if count > 1:
        @pl.loop(1, count)
        def _(j):
            finish(me * own + j * chunk)

    load.wait()
    width = nl.shape[1]
    w_mine = pl.ds(pl.multiple_of(me * width, width), width)
    w_other = pl.ds(pl.multiple_of(other * width, width), width)
    tile = 512
    for j in range(count):
        copy(j).wait_recv()

        @pl.loop(0, w.shape[1] // tile)
        def _(t):
            cols = pl.ds(pl.multiple_of(t * tile, tile), tile)
            held = nl[pl.ds(pl.multiple_of(me * own + j * chunk, chunk), chunk), :]
            y_ref[pl.ds(j * chunk, chunk), cols] = (
                dot(held, w[w_mine, cols]) + dot(nr[pl.ds(j * chunk, chunk), :], w[w_other, cols])
            ).astype(bf16)

    dec_copy.wait()
    held = dl[pl.ds(pl.multiple_of(me * PAD, PAD), PAD), :]
    yd_ref[...] = (dot(held, w[w_mine, :]) + dot(dr[...], w[w_other, :])).astype(bf16)
    for j in range(count):
        copy(j).wait_send()


def decode_kernel(heads, cols_ref, v_ref, s_ref, att_ref, new_ref):
    for h in range(heads):
        state = s_ref[0, h]
        qe = cols_ref[0, :, h : h + 1]
        e = cols_ref[0, :, heads + h : heads + h + 1]
        k = cols_ref[0, :, 2 * heads + h : 2 * heads + h + 1]
        qk = cols_ref[0, 0:1, 3 * heads + h : 3 * heads + h + 1]
        v = v_ref[0, :, h * DV : (h + 1) * DV]
        att_ref[0, :, h * DV : (h + 1) * DV] = jnp.sum(qe * state, axis=0, keepdims=True) + qk * v
        new_ref[0, h] = e * state + k * v


ANY = pl.BlockSpec(memory_space=pl.ANY)
VMEM = pl.BlockSpec(memory_space=pltpu.VMEM)
LIMIT = 60 * 1024 * 1024


def on_device(
    pieces, new_tokens, w_query, w_key, w_value, w_decay, decay_bias, norm_gain, head_gain, w_out, prompt_state, decode_state,
):
    kv_size = lax.axis_size("kv")
    tp_index = lax.axis_index("tp")
    kv_index = lax.axis_index("kv")
    qk = w_query.shape[1]
    heads = qk // DK
    vw = heads * DV
    own_pos, prompts, width = pieces.shape
    own = own_pos * prompts
    chunk = min(256, own)
    count = own // chunk
    rows = 2 * own
    dec_own = new_tokens.shape[0]
    bias_here = lax.dynamic_slice_in_dim(decay_bias, tp_index * qk, qk)[None]
    gain_here = lax.dynamic_slice_in_dim(head_gain, tp_index * vw, vw)[None]
    whole_start = lax.all_gather(prompt_state.astype(bf16), "kv", axis=2, tiled=True)
    whole_start = whole_start.transpose(1, 0, 3, 2).astype(f32)

    mats = jnp.asarray(sum_matrices(prompts), bf16)
    dec_rows = jnp.pad(new_tokens, ((0, PAD - dec_own), (0, 0)))
    proj_flops = 2 * rows * width * (3 * qk + vw)
    out_local, q_total, local, totals, dec_prod = pl.pallas_call(
        functools.partial(front_kernel, own, chunk, prompts, heads),
        name="front",
        out_shape=(
            jax.ShapeDtypeStruct((rows, vw), bf16),
            jax.ShapeDtypeStruct((rows, qk), bf16),
            jax.ShapeDtypeStruct((heads, prompts * DV, DK), f32),
            jax.ShapeDtypeStruct((8, qk), f32),
            jax.ShapeDtypeStruct((2 * PAD, 3 * qk + vw), f32),
        ),
        in_specs=[ANY, VMEM, ANY, ANY, ANY, ANY, VMEM, VMEM, VMEM],
        out_specs=(VMEM,) * 5,
        scratch_shapes=[
            pltpu.VMEM((own, width), bf16),
            pltpu.VMEM((rows, width), bf16),
            pltpu.VMEM((2 * PAD, width), bf16),
            pltpu.VMEM((width, qk), bf16),
            pltpu.VMEM((width, qk), bf16),
            pltpu.VMEM((width, vw), bf16),
            pltpu.VMEM((width, qk), bf16),
            pltpu.VMEM((rows, qk), bf16),
            pltpu.VMEM((rows, qk), bf16),
            pltpu.VMEM((rows, vw), bf16),
            pltpu.VMEM((rows, qk), f32),
            pltpu.SemaphoreType.DMA((count,)),
            pltpu.SemaphoreType.DMA((4,)),
            pltpu.SemaphoreType.DMA((count,)),
            pltpu.SemaphoreType.DMA((count,)),
            pltpu.SemaphoreType.DMA,
            pltpu.SemaphoreType.DMA,
        ],
        compiler_params=pltpu.CompilerParams(collective_id=0, has_side_effects=True, vmem_limit_bytes=LIMIT),
        cost_estimate=pl.CostEstimate(flops=proj_flops, bytes_accessed=20_000_000, transcendentals=0),
    )(pieces.reshape(own, width), dec_rows, w_query, w_key, w_value, w_decay, bias_here, norm_gain[None], mats)

    totals = totals[:prompts].reshape(prompts, heads, DK).transpose(1, 0, 2)[:, :, None]
    local = local.reshape(heads, prompts, DV, DK)
    all_local = lax.all_gather(local.astype(bf16), "kv")
    all_totals = lax.all_gather(totals, "kv")

    dec_all = dec_prod.reshape(2, PAD, -1)[:, :dec_own].reshape(2 * dec_own, -1)
    seqs = 2 * dec_own
    q_d = dec_all[:, :qk].reshape(seqs, heads, DK)
    k_d = dec_all[:, qk : 2 * qk].reshape(seqs, heads, DK)
    e_d = jnp.exp(dec_all[:, 2 * qk : 3 * qk]).reshape(seqs, heads, DK)
    qk_d = jnp.broadcast_to(jnp.sum(q_d * k_d, axis=-1, keepdims=True), q_d.shape)
    cols = jnp.concatenate([q_d * e_d, e_d, k_d, qk_d], axis=1).transpose(0, 2, 1)
    v_d = dec_all[:, 3 * qk :][:, None]
    dec_att, decode_out = pl.pallas_call(
        functools.partial(decode_kernel, heads),
        name="decode",
        grid=(seqs,),
        out_shape=(
            jax.ShapeDtypeStruct((seqs, 1, vw), f32),
            jax.ShapeDtypeStruct(decode_state.shape, f32),
        ),
        in_specs=[
            pl.BlockSpec((1, DK, 4 * heads), lambda i: (i, 0, 0)),
            pl.BlockSpec((1, 1, vw), lambda i: (i, 0, 0)),
            pl.BlockSpec((1, heads, DK, DV), lambda i: (i, 0, 0, 0)),
        ],
        out_specs=(
            pl.BlockSpec((1, 1, vw), lambda i: (i, 0, 0)),
            pl.BlockSpec((1, heads, DK, DV), lambda i: (i, 0, 0, 0)),
        ),
        cost_estimate=pl.CostEstimate(flops=8 * decode_state.size, bytes_accessed=8 * decode_state.size, transcendentals=0),
    )(cols, v_d, decode_state)

    running = whole_start
    incoming = whole_start
    for c in range(kv_size):
        incoming = jnp.where(kv_index == c, running, incoming)
        running = jnp.exp(all_totals[c]) * running + all_local[c].astype(f32)
    rows_k = prompt_state.shape[2]
    prompt_out = lax.dynamic_slice_in_dim(running, kv_index * rows_k, rows_k, 3).transpose(1, 0, 3, 2)

    dec_pad = jnp.pad(dec_att.reshape(2, dec_own, vw), ((0, 0), (0, PAD - dec_own), (0, 0))).reshape(2 * PAD, vw)
    y, yd = pl.pallas_call(
        functools.partial(back_kernel, own, chunk, prompts, heads),
        name="back",
        out_shape=(
            jax.ShapeDtypeStruct((own, w_out.shape[1]), bf16),
            jax.ShapeDtypeStruct((PAD, w_out.shape[1]), bf16),
        ),
        in_specs=[VMEM] * 5 + [ANY],
        out_specs=(VMEM,) * 2,
        scratch_shapes=[
            pltpu.VMEM(w_out.shape, bf16),
            pltpu.VMEM((rows, vw), bf16),
            pltpu.VMEM((own, vw), bf16),
            pltpu.VMEM((2 * PAD, vw), bf16),
            pltpu.VMEM((PAD, vw), bf16),
            pltpu.SemaphoreType.DMA,
            pltpu.SemaphoreType.DMA((count,)),
            pltpu.SemaphoreType.DMA((count,)),
            pltpu.SemaphoreType.DMA,
            pltpu.SemaphoreType.DMA,
        ],
        compiler_params=pltpu.CompilerParams(collective_id=1, has_side_effects=True, vmem_limit_bytes=LIMIT),
        cost_estimate=pl.CostEstimate(flops=2 * own * w_out.size, bytes_accessed=20_000_000, transcendentals=0),
    )(out_local, q_total, incoming.reshape(heads, prompts * DV, DK).astype(bf16), gain_here, dec_pad, w_out)
    return (y.reshape(own_pos, prompts, -1), yd[:dec_own], prompt_out, decode_out)


def solution(mesh):
    return jax.shard_map(
        on_device,
        mesh=mesh,
        in_specs=(
            P(("kv", "tp"), "dp", None),
            P(("dp", "kv", "tp"), None),
            P(None, "tp"),
            P(None, "tp"),
            P(None, "tp"),
            P(None, "tp"),
            P(),
            P(),
            P(),
            P(),
            P("dp", "tp", "kv", None),
            P(("dp", "kv"), "tp", None, None),
        ),
        out_specs=(
            P(("kv", "tp"), "dp", None),
            P(("dp", "kv", "tp"), None),
            P("dp", "tp", "kv", None),
            P(("dp", "kv"), "tp", None, None),
        ),
        check_vma=False,
    )
```

time: 604 us -> 182 us (0.30); the launches traced: 593 us -> 181 us
  local copies, waits for them, and re-layouts: 220 us -> 29.4 us
  other arithmetic: 163 us -> 5.34 us
  Pallas kernels: 0 us -> 95.4 us
  matrix products: 85 us -> 0 us
  waiting for transfers between devices: 68.3 us -> 0.02 us
    pallas_call x0 -> x3, Pallas kernels: none -> 95.4 us  [the longest x1 59.1 us: on_device(): pl.pallas_call(functools.partial(front_kernel, own, chunk, prompts, heads...]
    dot_general x39 -> x0, matrix products: 85 us -> none  [the longest x1 15.8 us: on_device(): jnp.einsum('ntbhk,nbhkv->ntbhv', start_queries.astype(jnp.float32), full_...]
    convert_element_type x57 -> x1, other arithmetic: 78.7 us -> 2.09 us  [on_device(): all_local = lax.all_gather(local.astype(bf16), 'kv')]
    all_gather x2 -> x1, waiting for transfers between devices: 56.6 us -> 0.01 us  [on_device(): all_local = lax.all_gather(local.astype(bf16), 'kv')]
    all_to_all x1 -> x0, local copies, waits for them, and re-layouts: 40.2 us -> none  [on_device(): lax.all_to_all(send_rows, 'tp', split_axis=0, concat_axis=2, tiled=True)]
    another operation x22 -> x0, local copies, waits for them, and re-layouts: 29.5 us -> none  [the longest x4 20.1 us: to_blocks(): return tensor.reshape((block_count, BLOCK) + tensor.shape[1:])]
    reshape x5 -> x6, local copies, waits for them, and re-layouts: 43.5 us -> 15.8 us  [the longest x1 7.65 us: on_device(): y.reshape(own_pos, prompts, -1)]
    another operation x17 -> x0, other arithmetic: 26.7 us -> none  [the longest x16 17.6 us: block_terms(): within = jnp.cumsum(g_blk, axis=0)]
  transfers between devices with their start and end apart: 3 -> 1, of which waited for: 3 -> 0; matrix products, arithmetic and copies ran while one was open for 7% -> 4% of each run, Pallas kernels for 0% -> 8%
where the time goes in v1:
time: 182 us; the launch traced here: 181 us
  Pallas kernels  95.4 us (52%)
  blocking collectives  36.5 us (20%)
  local copies, waits for them, and re-layouts  29.4 us (16%)
  between operations  14.3 us (8%)
  other arithmetic  5.34 us (3%)
    pallas_call x1, Pallas kernels, on_device(): pl.pallas_call(functools.partial(front_kernel, own, chunk, prompts, heads...  59.1 us
    pallas_call x1, Pallas kernels, on_device(): pl.pallas_call(functools.partial(back_kernel, own, chunk, prompts, heads)...  22 us
    all_gather x1, blocking collectives, on_device(): lax.all_gather(prompt_state.astype(bf16), 'kv', axis=2, tiled=True)  21.5 us
    all_gather x1, blocking collectives, on_device(): all_totals = lax.all_gather(totals, 'kv')  15 us
    pallas_call x1, Pallas kernels, on_device(): pl.pallas_call(functools.partial(decode_kernel, heads), name='decode', gr...  14.3 us
    reshape x1, local copies, waits for them, and re-layouts, on_device(): y.reshape(own_pos, prompts, -1)  7.65 us
    reshape x1, local copies, waits for them, and re-layouts, on_device(): pieces.reshape(own, width)  7.18 us
  transfers between devices with their start and end apart: 1, of which 0 were waited for; matrix products, arithmetic and copies ran while one was open for 4% of the time, Pallas kernels for 8%

profile of v1, /device:TPU:0, one launch (start us, length us, event | category | flops | bytes accessed | tf_op | source)
XLA Modules:
  0.0 180.9 jit_solution(9294594393646219178)
XLA Ops:
  7.2 0.0 all-gather.3.cloned.1.call-start
  7.2 0.0 copy-start.4
  7.2 0.0 copy-start.1
  7.2 7.2 %reshape.93.x_hbm = bf16[1024,2048]{1,0:T(8,128)(2,1)} reshape(bf16[512,2,2048]{2,1,0:T(2,128)(2,1)} %param.13) | data formatting | bytes 8388608 | tf_op jit(solution)/shard_map/reshape | solution.py:357
  14.4 0.0 copy-done.4
  14.4 0.7 dynamic_slice.9
  15.1 0.0 copy-done.1
  15.1 0.6 pad.8.dec_ref
  15.7 0.0 copy-start
  15.7 59.1 %front.1 = (bf16[2048,1024]{1,0:T(8,128)(2,1)}, bf16[2048,512]{1,0:T(8,128)(2,1)}, f32[4,512,128]{2,1,0:T(8,128)}, f32[8,512]{1,0:T(8,128)}, f32[32,2560]{1,0:T(8,128)}) custom-call(bf16[1024,2048]{1,0:T(8,128)(2,1)} %reshape.93.x_hbm, bf16[16,2048]{1,0:T(8,128)(2,1)} %pad.8.dec_ref, bf16[2048,512]{1,0:T(8,128)(2,1)} %wq_hbm.1, bf16[2048,512]{1,0:T(8,128)(2,1)} %wk_hbm.1, ...), custom_call_target="tpu_custom_call" | custom-call | flops 21474836480 | bytes 20000000 | tf_op jit(solution)/shard_map/front/pallas_call | solution.py:324
  74.8 2.1 %convert_element_type.58 = bf16[4,512,128]{2,1,0:T(8,128)(2,1)} convert(f32[4,512,128]{2,1,0:T(8,128)} %get-tuple-element.16) | non-fusion elementwise | flops 262144 | bytes 1572864 | tf_op jit(solution)/shard_map/convert_element_type | solution.py:361
  76.9 0.0 all-gather.3.cloned.1.call-update
  76.9 0.0 copy-done
  76.9 0.2 copy.72
  77.1 0.7 slice_bitcast_fusion.1
  77.8 15.0 %all-gather = f32[16,2,128]{2,1,0:T(2,128)S(1)} all-gather(f32[4,2,128]{2,1,0:T(2,128)S(1)} %slice_bitcast_fusion.1), channel_id=2, replica_groups=mesh['dp'=4,'kv'=4,'tp'=2] {'kv'}, dimensions={0}, use_global_device_ids=true | all-gather | bytes 20480 | tf_op jit(solution)/shard_map/all_gather | solution.py:362
  92.8 0.2 copy.46
  93.0 0.2 copy.42
  93.2 0.2 copy.54
  93.4 0.2 copy.44
  93.5 0.9 slice_bitcast_fusion
  94.5 0.7 broadcast_in_dim.22.v_ref
  95.3 0.1 fusion.6
  95.4 1.3 copy.52
  96.7 0.0 copy-start.3
  96.7 14.3 %decode.1 = (f32[16,1,1024]{2,1,0:T(1,128)}, f32[16,4,128,256]{3,2,1,0:T(8,128)}) custom-call(f32[16,128,16]{2,1,0:T(8,128)} %bitcast.64, f32[16,1,1024]{2,1,0:T(1,128)} %broadcast_in_dim.22.v_ref, f32[16,4,128,256]{3,2,1,0:T(8,128)} %s_ref.1), custom_call_target="tpu_custom_call" | custom-call | flops 16777216 | bytes 16777216 | tf_op jit(solution)/shard_map/decode/pallas_call | solution.py:372
  111.0 0.9 copy.73
  111.8 0.0 copy-done.3
  111.9 0.6 dynamic_slice.10
  112.5 0.7 pad.9
  113.1 0.6 constant_dynamic-slice_fusion
  113.7 21.5 %all_gather.11 = bf16[2,4,128,256]{3,1,0,2:T(4,128)(2,1)S(1)} all-gather(bf16[2,4,32,256]{3,1,0,2:T(4,128)(2,1)S(1)} %copy.72), channel_id=1, replica_groups=mesh['dp'=4,'kv'=4,'tp'=2] {'kv'}, dimensions={2}, use_global_device_ids=true | all-gather | bytes 655360 | tf_op jit(solution)/shard_map/all_gather | solution.py:318
  135.2 0.0 all-gather.3.cloned.1.call-done
  135.2 1.7 fusion.11
  136.9 0.4 copy.65
  137.3 0.4 copy.63
  137.7 0.4 copy.62
  138.2 0.4 copy.61
  138.6 2.2 %convert_add_fusion = (f32[4,2,256,128]{2,0,1,3:T(4,128)S(1)}, bf16[4,2,256,128]{2,0,1,3:T(4,128)(2,1)S(1)}) fusion(bf16[1,4,2,256,128]{3,1,2,4,0:T(4,128)(2,1)S(1)} %copy.63, bf16[1,4,2,256,128]{3,1,2,4,0:T(4,128)(2,1)S(1)} %copy.62, bf16[2,4,128,256]{3,1,0,2:T(4,128)(2,1)S(1)} %all_gather.11, bf16[1,4,2,256,128]{3,1,2,4,0:T(4,128)(2,1)S(1)} %copy.61, ...), kind=kLoop, calls=%fused_computation | loop fusion | flops 3670016 | bytes 3682307 | tf_op jit(solution)/shard_map/add | solution.py:396
  140.8 0.9 fusion.5
  141.7 0.8 copy.56
  142.5 1.2 copy.51
  143.7 22.0 %back.1 = (bf16[1024,2048]{1,0:T(8,128)(2,1)}, bf16[16,2048]{1,0:T(8,128)(2,1)}) custom-call(bf16[2048,1024]{1,0:T(8,128)(2,1)} %get-tuple-element.13.out_ref, bf16[2048,512]{1,0:T(8,128)(2,1)} %get-tuple-element.14.qt_ref, bf16[4,512,128]{2,1,0:T(8,128)(2,1)} %bitcast.67, f32[1,1024]{1,0:T(1,128)} %bitcast.71, f32[32,1024]{1,0:T(8,128)} %bitcast.69, ...), custom_call_target="tpu_custom_call" | custom-call | flops 8589934592 | bytes 20000000 | tf_op jit(solution)/shard_map/back/pallas_call | solution.py:401
  165.8 0.0 copy-start.2
  165.8 7.6 %reshape.102 = bf16[512,2,2048]{2,1,0:T(2,128)(2,1)} reshape(bf16[1024,2048]{1,0:T(8,128)(2,1)} %get-tuple-element.19) | data formatting | bytes 8388608 | tf_op jit(solution)/shard_map/reshape | solution.py:425
  173.4 0.0 copy-done.2
  173.4 0.6 slice.57
  (11 shorter events, 0.1 us)
Async XLA Ops:
  7.2 128.0 %all-gather.3.cloned.1.call-start = ((), (), s32[]{:S(2)}) async-start(), calls=%async_computation | async-start | bytes 2621440 | tf_op jit(solution)/shard_map/all_gather | solution.py:361
  7.2 7.2 %copy-start.4 = (f32[1024]{0:T(1024)S(1)}, f32[1024]{0:T(1024)}, u32[]{:S(2)}) copy-start(f32[1024]{0:T(1024)} %param.19) | copy-start | bytes 12292
  7.2 7.8 %copy-start.1 = (bf16[8,2048]{1,0:T(8,128)(2,1)S(1)}, bf16[8,2048]{1,0:T(8,128)(2,1)}, u32[]{:S(2)}) copy-start(bf16[8,2048]{1,0:T(8,128)(2,1)} %param.14) | copy-start | bytes 98308
  15.7 61.2 %copy-start = (f32[2,4,32,256]{3,2,1,0:T(8,128)S(1)}, f32[2,4,32,256]{3,2,1,0:T(8,128)}, u32[]{:S(2)}) copy-start(f32[2,4,32,256]{3,2,1,0:T(8,128)} %param.23) | copy-start | bytes 786436
  96.7 15.1 %copy-start.3 = (f32[2048]{0:T(1024)S(1)}, f32[2048]{0:T(1024)}, u32[]{:S(2)}) copy-start(f32[2048]{0:T(1024)} %param.21) | copy-start | bytes 24580
  165.8 7.7 %copy-start.2 = (bf16[16,2048]{1,0:T(8,128)(2,1)S(1)}, bf16[16,2048]{1,0:T(8,128)(2,1)}, u32[]{:S(2)}) copy-start(bf16[16,2048]{1,0:T(8,128)(2,1)} %get-tuple-element.20) | copy-start | bytes 196612
Sparse Core Ops, SparseCore 0:
  77.0 55.9 all-gather.2

commit v2 on v1

--- a/solution.py
+++ b/solution.py
@@ -315,8 +315,8 @@
     dec_own = new_tokens.shape[0]
     bias_here = lax.dynamic_slice_in_dim(decay_bias, tp_index * qk, qk)[None]
     gain_here = lax.dynamic_slice_in_dim(head_gain, tp_index * vw, vw)[None]
-    whole_start = lax.all_gather(prompt_state.astype(bf16), "kv", axis=2, tiled=True)
-    whole_start = whole_start.transpose(1, 0, 3, 2).astype(f32)
+    rows_k = prompt_state.shape[2]
+    start_here = prompt_state.astype(bf16).transpose(1, 0, 2, 3).reshape(heads, -1, DK)
 
     mats = jnp.asarray(sum_matrices(prompts), bf16)
     dec_rows = jnp.pad(new_tokens, ((0, PAD - dec_own), (0, 0)))
@@ -358,8 +358,22 @@
 
     totals = totals[:prompts].reshape(prompts, heads, DK).transpose(1, 0, 2)[:, :, None]
     local = local.reshape(heads, prompts, DV, DK)
-    all_local = lax.all_gather(local.astype(bf16), "kv")
-    all_totals = lax.all_gather(totals, "kv")
+    flat_totals = totals[:, :, 0]
+    total_hi = flat_totals.astype(bf16)
+    total_left = flat_totals - total_hi.astype(f32)
+    total_mid = total_left.astype(bf16)
+    total_low = (total_left - total_mid.astype(f32)).astype(bf16)
+    state_rows = prompts * DV
+    sent = jnp.concatenate(
+        [local.reshape(heads, state_rows, DK).astype(bf16), start_here, total_hi, total_mid, total_low], axis=1
+    )
+    moved = lax.all_gather(sent, "kv")
+    all_local = moved[:, :, :state_rows].reshape(kv_size, heads, prompts, DV, DK)
+    start_end = state_rows + start_here.shape[1]
+    whole_start = moved[:, :, state_rows:start_end].reshape(kv_size, heads, prompts, rows_k, DV)
+    whole_start = whole_start.transpose(1, 2, 4, 0, 3).reshape(heads, prompts, DV, DK).astype(f32)
+    terms = moved[:, :, start_end:].reshape(kv_size, heads, 3, prompts, DK).astype(f32)
+    all_totals = ((terms[:, :, 0] + terms[:, :, 1]) + terms[:, :, 2])[:, :, :, None]
 
     dec_all = dec_prod.reshape(2, PAD, -1)[:, :dec_own].reshape(2 * dec_own, -1)
     seqs = 2 * dec_own
@@ -394,7 +408,6 @@
     for c in range(kv_size):
         incoming = jnp.where(kv_index == c, running, incoming)
         running = jnp.exp(all_totals[c]) * running + all_local[c].astype(f32)
-    rows_k = prompt_state.shape[2]
     prompt_out = lax.dynamic_slice_in_dim(running, kv_index * rows_k, rows_k, 3).transpose(1, 0, 3, 2)
 
     dec_pad = jnp.pad(dec_att.reshape(2, dec_own, vw), ((0, 0), (0, PAD - dec_own), (0, 0))).reshape(2 * PAD, vw)

time: 182 us -> 202 us (1.11)
  waiting for transfers between devices: 0.02 us -> 38.5 us
  blocking collectives: 36.5 us -> 0 us
  local copies, waits for them, and re-layouts: 29.4 us -> 40.3 us
  other arithmetic: 5.34 us -> 12.1 us
    all_gather x1, waiting for transfers between devices: 0.01 us -> 38.5 us  [on_device(): moved = lax.all_gather(sent, 'kv')]
    all_gather x2 -> x0, blocking collectives: 36.5 us -> none  [the longest x1 21.5 us: on_device(): lax.all_gather(prompt_state.astype(bf16), 'kv', axis=2, tiled=True)]
    convert_element_type x1 -> x7, other arithmetic: 2.09 us -> 9.86 us  [the longest x2 3.35 us: on_device(): running = jnp.exp(all_totals[c]) * running + all_local[c].astype(f32)]
    convert_element_type x1 -> x7, local copies, waits for them, and re-layouts: 1.23 us -> 5.79 us  [the longest x5 4.4 us: on_device(): whole_start.transpose(1, 2, 4, 0, 3).reshape(heads, prompts, DV, DK)]
    dynamic_slice x1 -> x4, local copies, waits for them, and re-layouts: 0.62 us -> 4.94 us  [on_device(): lax.dynamic_slice_in_dim(running, kv_index * rows_k, rows_k, 3)]
    concatenate x0 -> x1, local copies, waits for them, and re-layouts: none -> 2.76 us  [on_device(): jnp.concatenate([local.reshape(heads, state_rows, DK).astype(bf16), start...]
    unnamed x17 -> x21, local copies, waits for them, and re-layouts: 3.55 us -> 5.63 us
  transfers between devices with their start and end apart: 1 -> 1, of which waited for: 0 -> 1; matrix products, arithmetic and copies ran while one was open for 4% -> 3% of each run, Pallas kernels for 8% -> 7%
where the time goes in v2:
time: 202 us; the launch traced here: 201 us
  Pallas kernels  95.4 us (47%)
  local copies, waits for them, and re-layouts  40.3 us (20%)
  waiting for transfers between devices  38.5 us (19%)
  between operations  14.3 us (7%)
  other arithmetic  12.1 us (6%)
    pallas_call x1, Pallas kernels, on_device(): pl.pallas_call(functools.partial(front_kernel, own, chunk, prompts, heads...  59 us
    all_gather x1, waiting for transfers between devices, on_device(): moved = lax.all_gather(sent, 'kv')  38.5 us
    pallas_call x1, Pallas kernels, on_device(): pl.pallas_call(functools.partial(back_kernel, own, chunk, prompts, heads)...  22 us
    pallas_call x1, Pallas kernels, on_device(): pl.pallas_call(functools.partial(decode_kernel, heads), name='decode', gr...  14.4 us
    reshape x1, local copies, waits for them, and re-layouts, on_device(): y.reshape(own_pos, prompts, -1)  7.76 us
    reshape x1, local copies, waits for them, and re-layouts, on_device(): pieces.reshape(own, width)  7.18 us
    unnamed x21, local copies, waits for them, and re-layouts  5.63 us
    dynamic_slice x4, local copies, waits for them, and re-layouts, on_device(): lax.dynamic_slice_in_dim(running, kv_index * rows_k, rows_k, 3)  4.94 us
  transfers between devices with their start and end apart: 1, of which 1 were waited for; matrix products, arithmetic and copies ran while one was open for 3% of the time, Pallas kernels for 7%

profile of v2, /device:TPU:0, one launch (start us, length us, event | category | flops | bytes accessed | tf_op | source)
XLA Modules:
  0.0 200.6 jit_solution(3045193397401159847)
XLA Ops:
  7.2 0.0 all-gather.3.cloned.1.call-start
  7.2 1.0 convert_bitcast_fusion
  8.3 0.0 copy-start.6
  8.3 0.0 copy-start.3
  8.3 7.2 %reshape.140.x_hbm = bf16[1024,2048]{1,0:T(8,128)(2,1)} reshape(bf16[512,2,2048]{2,1,0:T(2,128)(2,1)} %param.13) | data formatting | bytes 8388608 | tf_op jit(solution)/shard_map/reshape | solution.py:357
  15.5 0.0 copy-done.6
  15.5 0.7 dynamic_slice.9
  16.1 0.0 copy-done.3
  16.1 0.6 pad.8.dec_ref
  16.8 59.0 %front.1 = (bf16[2048,1024]{1,0:T(8,128)(2,1)}, bf16[2048,512]{1,0:T(8,128)(2,1)}, f32[4,512,128]{2,1,0:T(8,128)}, f32[8,512]{1,0:T(8,128)}, f32[32,2560]{1,0:T(8,128)}) custom-call(bf16[1024,2048]{1,0:T(8,128)(2,1)} %reshape.140.x_hbm, bf16[16,2048]{1,0:T(8,128)(2,1)} %pad.8.dec_ref, bf16[2048,512]{1,0:T(8,128)(2,1)} %wq_hbm.1, bf16[2048,512]{1,0:T(8,128)(2,1)} %wk_hbm.1, ...), custom_call_target="tpu_custom_call" | custom-call | flops 21474836480 | bytes 20000000 | tf_op jit(solution)/shard_map/front/pallas_call | solution.py:324
  75.8 0.8 subtract_convert_fusion
  76.6 1.3 convert_element_type.96
  77.9 2.8 %concatenate.6 = bf16[4,646,128]{2,1,0:T(8,128)(2,1)} concatenate(bf16[4,512,128]{2,1,0:T(8,128)(2,1)S(1)} %convert_element_type.96, bf16[4,128,128]{2,1,0:T(8,128)(2,1)S(1)} %reshape.141, bf16[4,2,128]{2,1,0:T(2,128)(2,1)S(1)} %get-tuple-element.24, bf16[4,2,128]{2,1,0:T(2,128)(2,1)S(1)} %get-tuple-element.23, bf16[4,2,128]{2,1,0:T(2,128)(2,1)S(1)} %get-tuple-element.22), dimensions={1} | concatenate | bytes 1323008 | tf_op jit(solution)/shard_map/concatenate | solution.py:367
  80.6 0.0 all-gather.3.cloned.1.call-update
  80.7 0.9 slice_bitcast_fusion
  81.6 0.7 broadcast_in_dim.23.v_ref
  82.4 0.1 fusion.9
  82.5 1.3 copy.63
  83.8 0.0 copy-start.5
  83.8 14.4 %decode.1 = (f32[16,1,1024]{2,1,0:T(1,128)}, f32[16,4,128,256]{3,2,1,0:T(8,128)}) custom-call(f32[16,128,16]{2,1,0:T(8,128)} %bitcast.90, f32[16,1,1024]{2,1,0:T(1,128)} %broadcast_in_dim.23.v_ref, f32[16,4,128,256]{3,2,1,0:T(8,128)} %s_ref.1), custom_call_target="tpu_custom_call" | custom-call | flops 16777216 | bytes 16777216 | tf_op jit(solution)/shard_map/decode/pallas_call | solution.py:386
  98.2 0.9 copy.79
  99.1 0.0 copy-done.5
  99.1 0.6 dynamic_slice.10
  99.7 0.7 pad.9
  100.3 38.5 %all-gather.3.cloned.1.call-done = bf16[16,646,128]{2,1,0:T(8,128)(2,1)} async-done(((bf16[4,646,128]{2,1,0:T(8,128)(2,1)}), bf16[16,646,128]{2,1,0:T(8,128)(2,1)}) %all-gather.3.cloned.1.call-update) | async-done | bytes 2646032 | tf_op jit(solution)/shard_map/all_gather | solution.py:370
  138.8 0.8 slice_convert_fusion.4
  139.6 1.1 slice_convert_fusion.3
  140.7 0.3 reshape.161
  141.0 0.8 copy.78
  141.8 1.1 copy.64
  143.0 0.8 reshape.152
  143.8 3.3 %slice_convert_fusion.2 = (f32[1,4,512,128]{3,2,1,0:T(8,128)S(1)}, bf16[1,4,512,128]{3,2,1,0:T(8,128)(2,1)S(1)}, f32[1,4,512,128]{3,2,1,0:T(8,128)}, f32[1,4,512,128]{3,2,1,0:T(8,128)}) fusion(bf16[4,4,646,128]{3,2,1,0:T(8,128)(2,1)} %bitcast.88), kind=kLoop, calls=%fused_computation.13 | loop fusion | flops 786432 | bytes 5767168 | tf_op jit(solution)/shard_map/convert_element_type | solution.py:410
  147.2 0.1 constant_dynamic-slice_fusion.4
  147.3 0.1 constant_dynamic-slice_fusion
  147.3 1.3 copy.61
  148.6 1.4 copy.65
  150.0 0.1 convert.14
  150.1 1.3 constant_dynamic-slice_fusion.5
  151.4 0.0 copy-start
  151.4 1.7 copy.75
  153.1 3.5 %constant_dynamic-slice_fusion.1 = (f32[4,2,256,32]{3,2,1,0:T(8,128)}, f32[4,2,256,32]{3,2,1,0:T(8,128)}) fusion(f32[4,2,256,128]{3,2,1,0:T(8,128)} %bitcast.91, s32[]{:T(128)S(6)} %select_n.42, f32[4,2,256,128]{3,2,1,0:T(8,128)} %bitcast.92), kind=kLoop, calls=%fused_computation.43 | loop fusion | bytes 1048580 | tf_op jit(solution)/shard_map/dynamic_slice | solution.py:411
  156.6 1.5 copy.74
  158.1 1.5 copy.73
  159.6 0.0 copy-done
  159.6 2.5 %fusion.2.in_ref = bf16[4,512,128]{2,1,0:T(8,128)(2,1)} fusion(f32[4,512,128]{2,1,0:T(8,128)} %copy.61, f32[4,2,128]{2,1,0:T(2,128)S(1)} %copy.72, f32[4,2,128]{2,1,0:T(2,128)S(1)} %copy.71, f32[4,2,128]{2,1,0:T(2,128)S(1)} %copy.70, pred[]{:T(512)S(6)} %eq.12, pred[]{:T(512)S(6)} %eq.11, pred[]{:T(512)S(6)} %eq.10, bf16[4,4,646,128]{3,2,1,0:T(8,128)(2,1)S(1)} %bitcast.89), kind=kLoop, calls=%fused_computation.4 | loop fusion | flops 3407872 | bytes 3158019 | tf_op jit(solution)/shard_map/convert_element_type | solution.py:437
  162.2 22.0 %back.1 = (bf16[1024,2048]{1,0:T(8,128)(2,1)}, bf16[16,2048]{1,0:T(8,128)(2,1)}) custom-call(bf16[2048,1024]{1,0:T(8,128)(2,1)} %get-tuple-element.13.out_ref, bf16[2048,512]{1,0:T(8,128)(2,1)} %get-tuple-element.14.qt_ref, bf16[4,512,128]{2,1,0:T(8,128)(2,1)} %fusion.2.in_ref, f32[1,1024]{1,0:T(1,128)} %bitcast.99, f32[32,1024]{1,0:T(8,128)} %bitcast.97, ...), custom_call_target="tpu_custom_call" | custom-call | flops 8589934592 | bytes 20000000 | tf_op jit(solution)/shard_map/back/pallas_call | solution.py:414
  184.2 0.0 copy-start.4
  184.2 0.0 copy-start.1
  184.2 0.0 copy-start.2
  184.2 7.8 %reshape.150 = bf16[512,2,2048]{2,1,0:T(2,128)(2,1)} reshape(bf16[1024,2048]{1,0:T(8,128)(2,1)} %get-tuple-element.19) | data formatting | bytes 8388608 | tf_op jit(solution)/shard_map/reshape | solution.py:438
  192.0 0.0 copy-done.4
  192.0 0.6 slice.94
  192.6 0.0 copy-done.1
  192.6 0.0 copy-done.2
  192.6 0.2 fusion
  192.8 0.9 fusion.8
  (15 shorter events, 0.2 us)
Async XLA Ops:
  7.2 131.6 %all-gather.3.cloned.1.call-start = ((), (), s32[]{:S(2)}) async-start(), calls=%async_computation | async-start | bytes 3317760 | tf_op jit(solution)/shard_map/all_gather | solution.py:370
  8.3 7.2 %copy-start.6 = (f32[1024]{0:T(1024)S(1)}, f32[1024]{0:T(1024)}, u32[]{:S(2)}) copy-start(f32[1024]{0:T(1024)} %param.19) | copy-start | bytes 12292
  8.3 7.8 %copy-start.3 = (bf16[8,2048]{1,0:T(8,128)(2,1)S(1)}, bf16[8,2048]{1,0:T(8,128)(2,1)}, u32[]{:S(2)}) copy-start(bf16[8,2048]{1,0:T(8,128)(2,1)} %param.14) | copy-start | bytes 98308
  83.8 15.2 %copy-start.5 = (f32[2048]{0:T(1024)S(1)}, f32[2048]{0:T(1024)}, u32[]{:S(2)}) copy-start(f32[2048]{0:T(1024)} %param.21) | copy-start | bytes 24580
  151.4 8.2 %copy-start = (bf16[16,646,128]{2,1,0:T(8,128)(2,1)S(1)}, bf16[16,646,128]{2,1,0:T(8,128)(2,1)}, u32[]{:S(2)}) copy-start(bf16[16,646,128]{2,1,0:T(8,128)(2,1)} %all-gather.3.cloned.1.call-done) | copy-start | bytes 7938052
  184.2 7.8 %copy-start.4 = (bf16[16,2048]{1,0:T(8,128)(2,1)S(1)}, bf16[16,2048]{1,0:T(8,128)(2,1)}, u32[]{:S(2)}) copy-start(bf16[16,2048]{1,0:T(8,128)(2,1)} %get-tuple-element.20) | copy-start | bytes 196612
  184.2 8.4 %copy-start.1 = (f32[4,2,256,4,32]{2,4,3,0,1:T(8,128)S(1)}, f32[4,2,256,4,32]{2,4,3,0,1:T(8,128)}, u32[]{:S(2)}) copy-start(f32[4,2,256,4,32]{2,4,3,0,1:T(8,128)} %copy.64) | copy-start | bytes 3145732
  184.2 8.4 %copy-start.2 = (f32[4,2,256,128]{2,3,0,1:T(8,128)S(1)}, f32[4,2,256,128]{2,3,0,1:T(8,128)}, u32[]{:S(2)}) copy-start(f32[4,2,256,128]{2,3,0,1:T(8,128)} %copy.65) | copy-start | bytes 3145732
Sparse Core Ops, SparseCore 0:
  80.8 57.9 all-gather.2
